TPU v7x, 32 devices: a whole 2x2x4 slice. The times are simulated.
32 devices in a mesh: sp: 8 (over z, x), tp: 4 (over y, core).
Axes of the slice: x: 2, y: 2, z: 4, core: 2. Of those that a mesh axis runs over, the one named last changes fastest.
Arguments:
- inputs: bfloat16 [8192, 2048], P('sp'), may hold values from -9 to 9
- w_query: bfloat16 [2048, 1024], P(None, 'tp'), may hold values from -0.15692044 to 0.15692044
- w_key: bfloat16 [2048, 1024], P(None, 'tp'), may hold values from -0.15692044 to 0.15692044
- w_value: bfloat16 [2048, 1024], P(None, 'tp'), may hold values from -0.125 to 0.125
- w_glu_value: bfloat16 [2048, 1024], P(None, 'tp'), may hold values from -0.37565048 to 0.37565048
- w_glu_gate: bfloat16 [2048, 1024], P(None, 'tp'), may hold values from -0.125 to 0.125
- conv_taps: float32 [31, 1024], P(None, 'tp'), may hold values from -4 to 4
- conv_gain: float32 [1024], P('tp'), may hold values from 0.1 to 1.9
- log_forget: float32 [8192, 8], P('sp', 'tp'), may hold values from -8192 to 0, as said below
- w_out: bfloat16 [2048, 2048], replicated, may hold values from -0.125 to 0.125
Outputs:
- result: bfloat16 [8192, 2048], P(('sp', 'tp'))
Inputs may be any that keep to these rules, and one draw needn't show every extreme that they name: `log_forget`: for each head, non-increasing along positions and at most zero.
All inputs are finite; a program needn't handle non-finite values.
Results may differ from a plain program's by a relative error of at most 0.014.
Values may be sent and summed in bfloat16 or wider, within the bound.
A program may use at most 128 MiB of HBM per device.

v0:
```python
import math
import jax
import jax.numpy as jnp
from jax import lax
from jax.sharding import PartitionSpec as P

HEAD_DIM = 128
NORM_EPS = 1e-05


def passed_along(value, axis, steps):
    count = lax.axis_size(axis)
    leading, last = (max(0, -steps), min(count, count - steps))
    return lax.ppermute(value, axis, [(source, source + steps) for source in range(leading, last)])


def on_device(
    inputs,
    w_query,
    w_key,
    w_value,
    w_glu_value,
    w_glu_gate,
    conv_taps,
    conv_gain,
    log_forget,
    w_out,
):
    tok_rows = inputs.shape[0]
    channels = w_glu_value.shape[1]
    heads_here = w_query.shape[1] // HEAD_DIM
    attn_width = heads_here * HEAD_DIM
    tp_count = lax.axis_size("tp")
    tp_place = lax.axis_index("tp")
    total_channels = channels * tp_count
    row_start = lax.axis_index("sp") * tok_rows
    last_row = row_start + tok_rows - 1
    glu_value = jnp.dot(inputs, w_glu_value, preferred_element_type=jnp.float32)
    glu_gate = jnp.dot(inputs, w_glu_gate, preferred_element_type=jnp.float32)
    gated = (glu_value * jax.nn.sigmoid(glu_gate)).astype(jnp.bfloat16)
    kernel = conv_taps.shape[0]
    halo_rows = passed_along(gated[tok_rows - (kernel - 1) :], "sp", 1)
    padded = jnp.concatenate([halo_rows, gated], axis=0).astype(jnp.float32)
    conv_sum = jnp.zeros((tok_rows, channels), jnp.float32)
    for offset in range(kernel):
        conv_sum = conv_sum + conv_taps[offset] * padded[offset : offset + tok_rows]
    mean_value = lax.psum(jnp.sum(conv_sum, axis=1), "tp") / total_channels
    centered = conv_sum - mean_value[:, None]
    spread = lax.psum(jnp.sum(centered * centered, axis=1), "tp") / total_channels
    conv_rows = jax.nn.silu(centered * lax.rsqrt(spread + NORM_EPS)[:, None] * conv_gain).astype(
        jnp.bfloat16
    )
    query_rows = jnp.dot(inputs, w_query, preferred_element_type=jnp.float32).astype(jnp.bfloat16)
    key_rows = jnp.dot(inputs, w_key, preferred_element_type=jnp.float32).astype(jnp.bfloat16)
    value_rows = jnp.dot(inputs, w_value, preferred_element_type=jnp.float32).astype(jnp.bfloat16)
    query_heads = query_rows.reshape(tok_rows, heads_here, HEAD_DIM)
    own_gates = jnp.transpose(log_forget)
    gates_all = lax.all_gather(log_forget, "sp", axis=0, tiled=True)
    score_scale = HEAD_DIM ** (-0.5)
    query_pos = row_start + jnp.arange(tok_rows, dtype=jnp.int32)
    start_state = (
        jnp.full((heads_here, tok_rows), -1e30, jnp.float32),
        jnp.zeros((heads_here, tok_rows), jnp.float32),
        jnp.zeros((heads_here, tok_rows, HEAD_DIM), jnp.float32),
    )
    piece_keys = lax.all_gather(key_rows, "sp", axis=0, tiled=True)
    piece_values = lax.all_gather(value_rows, "sp", axis=0, tiled=True)
    block_rows = math.gcd(piece_keys.shape[0], tok_rows)
    shards = piece_keys.shape[0] // block_rows
    key_iota = jnp.arange(block_rows, dtype=jnp.int32)

    def one_shard(shard_number, carried_state):
        offset = shard_number * block_rows
        key_first = offset

        def attend(state_in):
            running_max, running_sum, running_out = state_in
            shard_keys = lax.dynamic_slice_in_dim(piece_keys, offset, block_rows, 0).reshape(
                block_rows, heads_here, HEAD_DIM
            )
            shard_values = lax.dynamic_slice_in_dim(piece_values, offset, block_rows, 0).reshape(
                block_rows, heads_here, HEAD_DIM
            )
            shard_gates = jnp.transpose(
                lax.dynamic_slice_in_dim(gates_all, key_first, block_rows, 0)
            )
            scores = (
                jnp.einsum(
                    "qhd,khd->hqk", query_heads, shard_keys, preferred_element_type=jnp.float32
                )
                * score_scale
            )
            scores = scores + own_gates[:, :, None] - shard_gates[:, None, :]
            allowed = ((key_first + key_iota)[None, :] <= query_pos[:, None])[None]
            masked = jnp.where(allowed, scores, -1e30)
            new_max = jnp.maximum(running_max, jnp.max(masked, axis=2))
            weights = jnp.where(allowed, jnp.exp(masked - new_max[:, :, None]), 0.0)
            rescale = jnp.exp(running_max - new_max)
            new_sum = running_sum * rescale + jnp.sum(weights, axis=2)
            mixture = jnp.einsum(
                "hqk,khd->hqd",
                weights.astype(jnp.bfloat16),
                shard_values,
                preferred_element_type=jnp.float32,
            )
            new_out = running_out * rescale[:, :, None] + mixture
            return (new_max, new_sum, new_out)

        def keep_state(state_in):
            return state_in

        return lax.cond(key_first <= last_row, attend, keep_state, carried_state)

    final_max, final_sum, final_out = lax.fori_loop(0, shards, one_shard, start_state)
    attn_heads = (final_out / final_sum[:, :, None]).astype(jnp.bfloat16)
    attn_rows = jnp.transpose(attn_heads, (1, 0, 2)).reshape(tok_rows, attn_width)
    conv_weight = lax.dynamic_slice_in_dim(w_out, tp_place * channels, channels, 0)
    attn_weight = lax.dynamic_slice_in_dim(
        w_out, total_channels + tp_place * attn_width, attn_width, 0
    )
    projected = jnp.dot(conv_rows, conv_weight, preferred_element_type=jnp.float32)
    return lax.psum_scatter(
        (projected + jnp.dot(attn_rows, attn_weight, preferred_element_type=jnp.float32)).astype(
            jnp.bfloat16
        ),
        "tp",
        scatter_dimension=0,
        tiled=True,
    )


def solution(mesh):
    in_specs = (
        P("sp", None),
        P(None, "tp"),
        P(None, "tp"),
        P(None, "tp"),
        P(None, "tp"),
        P(None, "tp"),
        P(None, "tp"),
        P("tp"),
        P("sp", "tp"),
        P(),
    )
    out_specs = P(("sp", "tp"), None)
    return jax.shard_map(
        on_device, mesh=mesh, in_specs=in_specs, out_specs=out_specs, check_vma=False
    )
```

profile of v0, /device:TPU:0, one launch (start us, length us, event | category | flops | bytes accessed | tf_op | source)
XLA Modules:
  0.0 321.7 jit_solution(7589455608530308768)
XLA Ops:
  6.5 0.0 copy-start
  6.5 0.0 copy-start.6
  6.5 0.0 all-gather.3.cloned.1.call-start
  6.5 1.2 copy-done
  7.8 4.2 %convolution_convert_fusion.2 = bf16[1024,256]{1,0:T(8,128)(2,1)} fusion(bf16[1024,2048]{1,0:T(8,128)(2,1)} %param.14, bf16[2048,256]{1,0:T(8,128)(2,1)S(1)} %copy-done), kind=kOutput, calls=%fused_computation.30 | convolution fusion | flops 1074003968 | bytes 5767168 | tf_op jit(solution)/shard_map/dot_general | solution.py:54
  12.0 0.0 all-gather.3.cloned.1.call-update
  12.0 0.0 copy-start.7
  12.0 0.0 all-gather.5.cloned.1.call-start
  12.1 4.6 %convolution_convert_fusion = bf16[1024,256]{1,0:T(8,128)(2,1)} fusion(bf16[1024,2048]{1,0:T(8,128)(2,1)} %param.14, bf16[2048,256]{1,0:T(8,128)(2,1)} %param.17), kind=kOutput, calls=%fused_computation.28 | convolution fusion | flops 1074003968 | bytes 5767168 | tf_op jit(solution)/shard_map/dot_general | solution.py:55
  16.7 0.0 all-gather.5.cloned.1.call-update
  16.7 0.0 reduce-scatter.2.cloned.1.call-start
  16.8 0.0 copy-done.6
  16.8 0.0 copy-start.5
  16.8 3.6 %fusion.18 = f32[1024,256]{1,0:T(8,128)S(1)} fusion(bf16[1024,2048]{1,0:T(8,128)(2,1)} %param.14, bf16[2048,256]{1,0:T(8,128)(2,1)S(1)} %copy-done.6), kind=kOutput, calls=%fused_computation.26 | convolution fusion | flops 1074528256 | bytes 6291456 | tf_op jit(solution)/shard_map/dot_general | solution.py:39
  20.4 0.0 copy-done.7
  20.4 0.0 copy-done.5
  20.4 1.3 fusion.19
  21.7 0.0 copy-start.3
  21.7 0.0 copy-start.2
  21.7 4.9 %collective-permute-start = (bf16[30,256]{1,0:T(8,128)(2,1)S(1)}, bf16[30,256]{1,0:T(8,128)(2,1)S(1)}, u32[]{:S(2)}, u32[]{:S(2)}) collective-permute-start(bf16[30,256]{1,0:T(8,128)(2,1)S(1)} %slice.252), channel_id=1, source_target_pairs={{0,4},{4,8},{8,12},{12,16},{16,20},{20,24},{24,28},{1,5},{5,9},{9,... | collective-permute-start | bytes 46088 | tf_op jit(solution)/shard_map/ppermute | solution.py:14
  26.6 3.8 %convolution_convert_fusion.1 = bf16[1024,256]{0,1:T(8,128)(2,1)S(1)} fusion(bf16[1024,2048]{1,0:T(8,128)(2,1)} %param.14, bf16[2048,256]{1,0:T(8,128)(2,1)} %param.15), kind=kOutput, calls=%fused_computation.29 | convolution fusion | flops 1074003968 | bytes 5767168 | tf_op jit(solution)/shard_map/dot_general | solution.py:53
  30.4 0.3 copy.17
  30.7 0.0 copy-done.3
  30.8 0.0 copy-done.2
  30.8 31.8 %all_gather.10 = f32[8192,2]{0,1:T(2,128)S(1)} all-gather(f32[1024,2]{0,1:T(2,128)S(1)} %copy-done.2), channel_id=1, replica_groups=mesh['sp'=8,'tp'=4] {'sp'}, dimensions={0}, use_global_device_ids=true | all-gather | bytes 73728 | tf_op jit(solution)/shard_map/all_gather | solution.py:58
  62.6 0.0 collective-permute-done
  62.6 0.1 maximum_convert_fusion
  62.7 0.0 copy-start.4
  62.7 4.3 %fusion.60 = (f32[1024]{0:T(1024)S(1)}, f32[1024,256]{1,0:T(8,128)S(1)}) fusion(f32[1054,256]{1,0:T(8,128)S(1)} %maximum_convert_fusion, f32[256]{0:T(256)S(1)} %bitcast.80, f32[256]{0:T(256)S(1)} %bitcast.81, f32[256]{0:T(256)S(1)} %bitcast.83, f32[256]{0:T(256)S(1)} %bitcast.84, f32[256]{0:T(256)S(1)} %bitcast.85, f32[256]{0:T(256)S(1)} %bitcast.86, ...), kind=kLoop, calls=%fused_computation.108 | loop fusion | flops 16251904 | bytes 33590272 | tf_op jit(solution)/shard_map/reduce_sum | solution.py:47
  67.1 6.1 %psum.14 = f32[1024]{0:T(1024)S(1)} all-reduce(f32[1024]{0:T(1024)S(1)} %get-tuple-element.333), channel_id=1, replica_groups=mesh['sp'=8,'tp'=4] {'tp'}, use_global_device_ids=true, to_apply=%region_1.0 | all-reduce | flops 1024 | bytes 8192 | tf_op jit(solution)/shard_map/psum | solution.py:47
  73.2 0.4 multiply_reduce_fusion
  73.5 6.6 %psum.15 = f32[1024]{0:T(1024)S(1)} all-reduce(f32[1024]{0:T(1024)S(1)} %multiply_reduce_fusion), channel_id=1, replica_groups=mesh['sp'=8,'tp'=4] {'tp'}, use_global_device_ids=true, to_apply=%region_3.0 | all-reduce | flops 1024 | bytes 8192 | tf_op jit(solution)/shard_map/psum | solution.py:49
  80.2 0.0 copy-done.4
  80.2 5.8 %fusion.51 = f32[1024,2048]{1,0:T(8,128)} fusion(bf16[2048,2048]{1,0:T(8,128)(2,1)} %param.23, s32[]{:T(128)S(6)} %select_n.18, f32[1024,256]{1,0:T(8,128)S(1)} %get-tuple-element.334, f32[256]{0:T(256)S(1)} %copy-done.4, f32[1024]{0:T(1024)S(1)} %add_rsqrt_fusion, f32[1024]{0:T(1024)S(1)} %broadcast_multiply_fusion), kind=kOutput, calls=%fused_computation.94 | convolution fusion | flops 1075838976 | bytes 10494980 | tf_op jit(solution)/shard_map/dot_general | solution.py:121
  86.0 2.5 all-gather.3.cloned.1.call-done
  88.5 6.4 %copy.16 = bf16[8192,256]{0,1:T(8,128)(2,1)} copy(bf16[8192,256]{1,0:T(8,128)(2,1)} %all-gather.3.cloned.1.call-done) | data formatting | bytes 8388608
  94.9 67.2 %all-gather.5.cloned.1.call-done = bf16[8192,256]{1,0:T(8,128)(2,1)} async-done(((bf16[1024,256]{1,0:T(8,128)(2,1)}), bf16[8192,256]{1,0:T(8,128)(2,1)}) %all-gather.5.cloned.1.call-update) | async-done | bytes 4194320 | tf_op jit(solution)/shard_map/all_gather | solution.py:67
  162.1 6.4 %copy.18 = bf16[8192,256]{0,1:T(8,128)(2,1)} copy(bf16[8192,256]{1,0:T(8,128)(2,1)} %all-gather.5.cloned.1.call-done) | data formatting | bytes 8388608
  168.5 0.1 broadcast_in_dim.40
  168.6 12.4 %while.18 = (s32[]{:T(128)}, f32[2,1024]{1,0:T(2,128)S(1)}, f32[2,1024]{1,0:T(2,128)S(1)}, f32[2,1024,128]{2,1,0:T(8,128)S(1)}, s32[]{:T(128)}, /*index=5*/bf16[...) while((s32[]{:T(128)}, f32[2,1024]{1,0:T(2,128)S(1)}, ...), condition=%wide.region_9.10_spmd.clone, body=%wide.region_4.9_spmd.clone.sunk | while | flops 1115166720 | bytes 35352928 | solution.py:114
  168.6 11.9 %conditional.3 = ((f32[2,1024]{1,0:T(2,128)S(1)}, f32[2,1024]{1,0:T(2,128)S(1)}, f32[2,1024,128]{2,1,0:T(8,128)S(1)})) conditional(s32[]{:T(128)} %convert_element_type.57, (f32[2,1024]{1,0:T(2,128)S(1)}, f32[2,1024]{1,0:T(2,128)S(1)}, f32[2,1024,128]{2,1,0:T(8,128)S(1)}) %tuple.78, (s32[]{:T(128)}, s32[1024]{0:T(1024)S(1)}, s32[]{:T(128)}, ...), branch_computations={%region_5.5_spmd, %region_6.8_spmd} | conditional | flops 1115166720 | bytes 35348560 | solution.py:112
  168.7 1.3 constant_dynamic-slice_fusion
  170.0 0.7 broadcast_compare_fusion
  170.6 2.6 fusion.6
  173.3 3.0 fusion.5
  176.3 4.2 %fusion.10 = f32[2,1024,128]{2,1,0:T(8,128)S(1)} fusion(bf16[1024,2,128]{0,2,1:T(8,128)(2,1)S(1)} %bitcast.65, f32[2,1024,1024]{2,1,0:T(8,128)S(1)} %get-tuple-element.336, f32[2,1024]{1,0:T(2,128)S(1)} %max.2, f32[2,1024]{1,0:T(2,128)S(1)} %dynamic-slice_bitcast_fusion, f32[2,1024]{1,0:T(2,128)S(1)} %get-tuple-element.230, ...), kind=kOutput, calls=%fused_computation.10 | convolution fusion | flops 552075264 | bytes 12091392 | tf_op jit(solution)/shard_map/while/body/eval_jaxpr/cond/branch_1_fun/hqk,khd->hqd/dot_general | solution.py:100
  181.0 0.3 copy.19
  181.3 0.1 divide_convert_fusion
  181.4 0.0 copy-start.1
  181.4 7.1 %add_convert_fusion = bf16[1024,2048]{1,0:T(8,128)(2,1)} fusion(f32[1024,2048]{1,0:T(8,128)} %fusion.51, bf16[1024,256]{0,1:T(8,128)(2,1)S(1)} %bitcast.67, bf16[2048,2048]{1,0:T(8,128)(2,1)} %param.23, s32[]{:T(128)S(6)} %select_n.19), kind=kOutput, calls=%fused_computation.21 | convolution fusion | flops 1077936128 | bytes 14155780 | tf_op jit(solution)/shard_map/dot_general | solution.py:123
  188.5 0.0 reduce-scatter.2.cloned.1.call-update
  188.5 126.7 %reduce-scatter.2.cloned.1.call-done = bf16[256,2048]{1,0:T(8,128)(2,1)} async-done(((bf16[1024,2048]{1,0:T(8,128)(2,1)}), bf16[256,2048]{1,0:T(8,128)(2,1)}) %reduce-scatter.2.cloned.1.call-update) | async-done | bytes 1048592 | tf_op jit(solution)/shard_map/reduce_scatter | solution.py:122
  315.2 0.0 copy-done.1
  (27 shorter events, 0.2 us)
Async XLA Ops:
  6.5 1.2 copy-start
  6.5 10.3 %copy-start.6 = (bf16[2048,256]{1,0:T(8,128)(2,1)S(1)}, bf16[2048,256]{1,0:T(8,128)(2,1)}, u32[]{:S(2)}) copy-start(bf16[2048,256]{1,0:T(8,128)(2,1)} %param.19) | copy-start | bytes 3145732
  6.5 81.9 %all-gather.3.cloned.1.call-start = ((), (), s32[]{:S(2)}) async-start(), calls=%async_computation.1 | async-start | bytes 4718592 | tf_op jit(solution)/shard_map/all_gather | solution.py:66
  12.0 8.4 %copy-start.7 = (bf16[2048,256]{1,0:T(8,128)(2,1)S(1)}, bf16[2048,256]{1,0:T(8,128)(2,1)}, u32[]{:S(2)}) copy-start(bf16[2048,256]{1,0:T(8,128)(2,1)} %param.18) | copy-start | bytes 3145732
  12.0 150.1 %all-gather.5.cloned.1.call-start = ((), (), s32[]{:S(2)}) async-start(), calls=%async_computation.2 | async-start | bytes 4718592 | tf_op jit(solution)/shard_map/all_gather | solution.py:67
  16.7 298.5 %reduce-scatter.2.cloned.1.call-start = ((), (), s32[]{:S(2)}) async-start(), calls=%async_computation.3 | async-start | bytes 5242880 | tf_op jit(solution)/shard_map/reduce_scatter | solution.py:122
  16.8 3.6 %copy-start.5 = (bf16[1024,2048]{1,0:T(8,128)(2,1)S(1)}, bf16[1024,2048]{1,0:T(8,128)(2,1)}, u32[]{:S(2)}) copy-start(bf16[1024,2048]{1,0:T(8,128)(2,1)} %param.14) | copy-start | bytes 12582916
  21.7 9.0 %copy-start.3 = (f32[31,256]{1,0:T(8,128)S(1)}, f32[31,256]{1,0:T(8,128)}, u32[]{:S(2)}) copy-start(f32[31,256]{1,0:T(8,128)} %param.20) | copy-start | bytes 95236
  21.7 9.1 %copy-start.2 = (f32[1024,2]{0,1:T(2,128)S(1)}, f32[1024,2]{0,1:T(2,128)}, u32[]{:S(2)}) copy-start(f32[1024,2]{0,1:T(2,128)} %param.22) | copy-start | bytes 24580
  21.7 40.9 %collective-permute-start = (bf16[30,256]{1,0:T(8,128)(2,1)S(1)}, bf16[30,256]{1,0:T(8,128)(2,1)S(1)}, u32[]{:S(2)}, u32[]{:S(2)}) collective-permute-start(bf16[30,256]{1,0:T(8,128)(2,1)S(1)} %slice.252), channel_id=1, source_target_pairs={{0,4},{4,8},{8,12},{12,16},{16,20},{20,24},{24,28},{1,5},{5,9},{9,... | collective-permute-start | bytes 46088 | tf_op jit(solution)/shard_map/ppermute | solution.py:14
  62.7 17.4 %copy-start.4 = (f32[256]{0:T(256)S(1)}, f32[256]{0:T(256)}, u32[]{:S(2)}) copy-start(f32[256]{0:T(256)} %param.21) | copy-start | bytes 3076
  181.4 133.8 %copy-start.1 = (bf16[2048,256]{1,0:T(8,128)(2,1)S(1)}, bf16[2048,256]{1,0:T(8,128)(2,1)}, u32[]{:S(2)}) copy-start(bf16[2048,256]{1,0:T(8,128)(2,1)} %param.16) | copy-start | bytes 3145732
Sparse Core Ops, SparseCore 0:
  12.1 76.2 all-gather.2
  90.6 71.4 all-gather.4
  188.6 126.5 reduce-scatter.1
where the time goes:
time: 322 us
  waiting for transfers between devices  196 us (61%)
  blocking collectives  44.5 us (14%)
  matrix products  37.3 us (12%)
  local copies, waits for them, and re-layouts  16.1 us (5%)
  between operations  13.3 us (4%)
  other arithmetic  8.6 us (3%)
  starting transfers between devices  4.96 us (2%)
    reduce_scatter x1, waiting for transfers between devices, on_device(): lax.psum_scatter((projected + jnp.dot(attn_rows, attn_weight, preferred_e...  127 us
    all_gather x1, waiting for transfers between devices, on_device(): piece_values = lax.all_gather(value_rows, 'sp', axis=0, tiled=True)  67.2 us
    all_gather x1, blocking collectives, on_device(): gates_all = lax.all_gather(log_forget, 'sp', axis=0, tiled=True)  31.8 us
    unnamed x19, local copies, waits for them, and re-layouts  14.3 us
    dot_general x1, matrix products, on_device(): jnp.dot(attn_rows, attn_weight, preferred_element_type=jnp.float32)  7.05 us
    psum x1, blocking collectives, on_device(): lax.psum(jnp.sum(centered * centered, axis=1), 'tp') / total_channels  6.63 us
  transfers between devices with their start and end apart: 4, of which 3 were waited for; matrix products, arithmetic and copies ran while one was open for 10% of the time, Pallas kernels for 0%

commit v1 on v0

--- a/solution.py
+++ b/solution.py
@@ -63,8 +63,11 @@
         jnp.zeros((heads_here, tok_rows), jnp.float32),
         jnp.zeros((heads_here, tok_rows, HEAD_DIM), jnp.float32),
     )
-    piece_keys = lax.all_gather(key_rows, "sp", axis=0, tiled=True)
-    piece_values = lax.all_gather(value_rows, "sp", axis=0, tiled=True)
+    piece_keys, piece_values = jnp.split(
+        lax.all_gather(jnp.concatenate([key_rows, value_rows], axis=1), "sp", axis=0, tiled=True),
+        [key_rows.shape[1]],
+        axis=1,
+    )
     block_rows = math.gcd(piece_keys.shape[0], tok_rows)
     shards = piece_keys.shape[0] // block_rows
     key_iota = jnp.arange(block_rows, dtype=jnp.int32)

time: 322 us -> 301 us (0.935)
  waiting for transfers between devices: 196 us -> 184 us
  local copies, waits for them, and re-layouts: 16.1 us -> 9.2 us
  matrix products: 37.3 us -> 33.8 us
    unnamed x19 -> x21, local copies, waits for them, and re-layouts: 14.3 us -> 1.54 us
    all_gather x2 -> x1, waiting for transfers between devices: 69.7 us -> 57.6 us  [on_device(): lax.all_gather(jnp.concatenate([key_rows, value_rows], axis=1), 'sp', axi...]
    split x0 -> x1, local copies, waits for them, and re-layouts: none -> 5.9 us  [on_device(): jnp.split(lax.all_gather(jnp.concatenate([key_rows, value_rows], axis=1),...]
    dot_general x1, matrix products: 4.63 us -> 1.29 us  [on_device(): jnp.dot(inputs, w_value, preferred_element_type=jnp.float32)]
  transfers between devices with their start and end apart: 4 -> 3, of which waited for: 3 -> 2; matrix products, arithmetic and copies ran while one was open for 10% -> 7% of each run, Pallas kernels for 0% -> 0%
where the time goes in v1:
time: 301 us
  waiting for transfers between devices  184 us (61%)
  blocking collectives  45.1 us (15%)
  matrix products  33.8 us (11%)
  between operations  13.7 us (5%)
  other arithmetic  9.64 us (3%)
  local copies, waits for them, and re-layouts  9.2 us (3%)
  starting transfers between devices  4.91 us (2%)
    reduce_scatter x1, waiting for transfers between devices, on_device(): lax.psum_scatter((projected + jnp.dot(attn_rows, attn_weight, preferred_e...  126 us
    all_gather x1, waiting for transfers between devices, on_device(): lax.all_gather(jnp.concatenate([key_rows, value_rows], axis=1), 'sp', axi...  57.6 us
    all_gather x1, blocking collectives, on_device(): gates_all = lax.all_gather(log_forget, 'sp', axis=0, tiled=True)  32.5 us
    dot_general x1, matrix products, on_device(): jnp.dot(attn_rows, attn_weight, preferred_element_type=jnp.float32)  7.05 us
    psum x1, blocking collectives, on_device(): lax.psum(jnp.sum(centered * centered, axis=1), 'tp') / total_channels  6.93 us
  transfers between devices with their start and end apart: 3, of which 2 were waited for; matrix products, arithmetic and copies ran while one was open for 7% of the time, Pallas kernels for 0%

profile of v1, /device:TPU:0, one launch (start us, length us, event | category | flops | bytes accessed | tf_op | source)
XLA Modules:
  0.0 300.7 jit_solution(1171972995764183568)
XLA Ops:
  6.5 0.0 copy-start
  6.5 0.0 copy-start.7
  6.5 0.0 all-gather.2.cloned.1.call-start
  6.5 1.2 copy-done
  7.8 0.0 copy-start.5
  7.8 3.6 %convolution_convert_fusion.2 = bf16[1024,256]{0,1:T(8,128)(2,1)S(1)} fusion(bf16[1024,2048]{1,0:T(8,128)(2,1)} %param.14, bf16[2048,256]{1,0:T(8,128)(2,1)S(1)} %copy-done), kind=kOutput, calls=%fused_computation.30 | convolution fusion | flops 1074003968 | bytes 5767168 | tf_op jit(solution)/shard_map/dot_general | solution.py:54
  11.4 0.0 copy-done.7
  11.4 0.0 copy-done.5
  11.4 0.0 copy-start.8
  11.4 1.3 convolution_convert_fusion.1
  12.7 0.0 copy-start.9
  12.7 1.0 pad_maximum_fusion
  13.8 0.0 all-gather.2.cloned.1.call-update
  13.8 0.0 reduce-scatter.2.cloned.1.call-start
  13.9 0.0 copy-done.8
  13.9 0.0 copy-start.6
  13.9 3.6 %fusion.18 = f32[1024,256]{1,0:T(8,128)S(1)} fusion(bf16[1024,2048]{1,0:T(8,128)(2,1)} %param.14, bf16[2048,256]{1,0:T(8,128)(2,1)S(1)} %copy-done.8), kind=kOutput, calls=%fused_computation.26 | convolution fusion | flops 1074528256 | bytes 6291456 | tf_op jit(solution)/shard_map/dot_general | solution.py:39
  17.5 0.0 copy-done.9
  17.5 0.0 copy-done.6
  17.5 1.3 fusion.19
  18.8 0.0 copy-start.3
  18.8 0.0 copy-start.2
  18.8 4.9 %collective-permute-start = (bf16[30,256]{1,0:T(8,128)(2,1)S(1)}, bf16[30,256]{1,0:T(8,128)(2,1)S(1)}, u32[]{:S(2)}, u32[]{:S(2)}) collective-permute-start(bf16[30,256]{1,0:T(8,128)(2,1)S(1)} %slice.252), channel_id=1, source_target_pairs={{0,4},{4,8},{8,12},{12,16},{16,20},{20,24},{24,28},{1,5},{5,9},{9,... | collective-permute-start | bytes 46088 | tf_op jit(solution)/shard_map/ppermute | solution.py:14
  23.7 4.3 %convolution_convert_fusion = bf16[1024,256]{0,1:T(8,128)(2,1)S(1)} fusion(bf16[1024,2048]{1,0:T(8,128)(2,1)} %param.14, bf16[2048,256]{1,0:T(8,128)(2,1)} %param.15), kind=kOutput, calls=%fused_computation.28 | convolution fusion | flops 1074003968 | bytes 5767168 | tf_op jit(solution)/shard_map/dot_general | solution.py:53
  28.0 0.3 copy.18
  28.3 0.0 copy-done.3
  28.3 0.0 copy-done.2
  28.3 32.5 %all_gather.7 = f32[8192,2]{0,1:T(2,128)S(1)} all-gather(f32[1024,2]{0,1:T(2,128)S(1)} %copy-done.2), channel_id=1, replica_groups=mesh['sp'=8,'tp'=4] {'sp'}, dimensions={0}, use_global_device_ids=true | all-gather | bytes 73728 | tf_op jit(solution)/shard_map/all_gather | solution.py:58
  60.9 0.0 collective-permute-done
  60.9 0.1 maximum_convert_fusion
  61.0 0.0 copy-start.4
  61.0 4.3 %fusion.60 = (f32[1024]{0:T(1024)S(1)}, f32[1024,256]{1,0:T(8,128)S(1)}) fusion(f32[1054,256]{1,0:T(8,128)S(1)} %maximum_convert_fusion, f32[256]{0:T(256)S(1)} %bitcast.80, f32[256]{0:T(256)S(1)} %bitcast.81, f32[256]{0:T(256)S(1)} %bitcast.83, f32[256]{0:T(256)S(1)} %bitcast.84, f32[256]{0:T(256)S(1)} %bitcast.85, f32[256]{0:T(256)S(1)} %bitcast.86, ...), kind=kLoop, calls=%fused_computation.109 | loop fusion | flops 16251904 | bytes 33590272 | tf_op jit(solution)/shard_map/reduce_sum | solution.py:47
  65.3 5.7 %psum.14 = f32[1024]{0:T(1024)S(1)} all-reduce(f32[1024]{0:T(1024)S(1)} %get-tuple-element.333), channel_id=1, replica_groups=mesh['sp'=8,'tp'=4] {'tp'}, use_global_device_ids=true, to_apply=%region_1.0 | all-reduce | flops 1024 | bytes 8192 | tf_op jit(solution)/shard_map/psum | solution.py:47
  71.0 0.4 multiply_reduce_fusion
  71.4 6.9 %psum.15 = f32[1024]{0:T(1024)S(1)} all-reduce(f32[1024]{0:T(1024)S(1)} %multiply_reduce_fusion), channel_id=1, replica_groups=mesh['sp'=8,'tp'=4] {'tp'}, use_global_device_ids=true, to_apply=%region_3.0 | all-reduce | flops 1024 | bytes 8192 | tf_op jit(solution)/shard_map/psum | solution.py:49
  78.3 0.0 copy-done.4
  78.3 5.8 %fusion.51 = f32[1024,2048]{1,0:T(8,128)} fusion(bf16[2048,2048]{1,0:T(8,128)(2,1)} %param.23, s32[]{:T(128)S(6)} %select_n.18, f32[1024,256]{1,0:T(8,128)S(1)} %get-tuple-element.334, f32[256]{0:T(256)S(1)} %copy-done.4, f32[1024]{0:T(1024)S(1)} %add_rsqrt_fusion, f32[1024]{0:T(1024)S(1)} %broadcast_multiply_fusion), kind=kOutput, calls=%fused_computation.95 | convolution fusion | flops 1075838976 | bytes 10494980 | tf_op jit(solution)/shard_map/dot_general | solution.py:124
  84.1 57.6 %all-gather.2.cloned.1.call-done = bf16[8192,512]{0,1:T(8,128)(2,1)} async-done(((bf16[1024,512]{0,1:T(8,128)(2,1)}), bf16[8192,512]{0,1:T(8,128)(2,1)}) %all-gather.2.cloned.1.call-update) | async-done | bytes 8388624 | tf_op jit(solution)/shard_map/all_gather | solution.py:67
  141.8 5.9 %fusion.62 = (bf16[8192,256]{0,1:T(8,128)(2,1)}, bf16[8192,256]{0,1:T(8,128)(2,1)}) fusion(bf16[8192,512]{0,1:T(8,128)(2,1)} %all-gather.2.cloned.1.call-done), kind=kLoop, calls=%fused_computation.110 | loop fusion | bytes 16777216 | tf_op jit(solution)/shard_map/split | solution.py:66
  147.7 0.1 broadcast_in_dim.40
  147.7 12.4 %while.18 = (s32[]{:T(128)}, f32[2,1024]{1,0:T(2,128)S(1)}, f32[2,1024]{1,0:T(2,128)S(1)}, f32[2,1024,128]{2,1,0:T(8,128)S(1)}, s32[]{:T(128)}, /*index=5*/bf16[...) while((s32[]{:T(128)}, f32[2,1024]{1,0:T(2,128)S(1)}, ...), condition=%wide.region_9.10_spmd.clone, body=%wide.region_4.9_spmd.clone.sunk | while | flops 1115166720 | bytes 35352928 | solution.py:117
  147.8 11.9 %conditional.3 = ((f32[2,1024]{1,0:T(2,128)S(1)}, f32[2,1024]{1,0:T(2,128)S(1)}, f32[2,1024,128]{2,1,0:T(8,128)S(1)})) conditional(s32[]{:T(128)} %convert_element_type.57, (f32[2,1024]{1,0:T(2,128)S(1)}, f32[2,1024]{1,0:T(2,128)S(1)}, f32[2,1024,128]{2,1,0:T(8,128)S(1)}) %tuple.79, (s32[]{:T(128)}, s32[1024]{0:T(1024)S(1)}, s32[]{:T(128)}, ...), branch_computations={%region_5.5_spmd, %region_6.8_spmd} | conditional | flops 1115166720 | bytes 35348560 | solution.py:115
  147.8 1.3 constant_dynamic-slice_fusion
  149.1 0.7 broadcast_compare_fusion
  149.8 2.6 fusion.6
  152.4 3.0 fusion.5
  155.5 4.2 %fusion.10 = f32[2,1024,128]{2,1,0:T(8,128)S(1)} fusion(bf16[1024,2,128]{0,2,1:T(8,128)(2,1)S(1)} %bitcast.65, f32[2,1024,1024]{2,1,0:T(8,128)S(1)} %get-tuple-element.336, f32[2,1024]{1,0:T(2,128)S(1)} %max.2, f32[2,1024]{1,0:T(2,128)S(1)} %dynamic-slice_bitcast_fusion, f32[2,1024]{1,0:T(2,128)S(1)} %get-tuple-element.230, ...), kind=kOutput, calls=%fused_computation.10 | convolution fusion | flops 552075264 | bytes 12091392 | tf_op jit(solution)/shard_map/while/body/eval_jaxpr/cond/branch_1_fun/hqk,khd->hqd/dot_general | solution.py:103
  160.1 0.3 copy.19
  160.5 0.1 divide_convert_fusion
  160.6 0.0 copy-start.1
  160.6 7.1 %add_convert_fusion = bf16[1024,2048]{1,0:T(8,128)(2,1)} fusion(f32[1024,2048]{1,0:T(8,128)} %fusion.51, bf16[1024,256]{0,1:T(8,128)(2,1)S(1)} %bitcast.67, bf16[2048,2048]{1,0:T(8,128)(2,1)} %param.23, s32[]{:T(128)S(6)} %select_n.19), kind=kOutput, calls=%fused_computation.21 | convolution fusion | flops 1077936128 | bytes 14155780 | tf_op jit(solution)/shard_map/dot_general | solution.py:126
  167.6 0.0 reduce-scatter.2.cloned.1.call-update
  167.7 126.2 %reduce-scatter.2.cloned.1.call-done = bf16[256,2048]{1,0:T(8,128)(2,1)} async-done(((bf16[1024,2048]{1,0:T(8,128)(2,1)}), bf16[256,2048]{1,0:T(8,128)(2,1)}) %reduce-scatter.2.cloned.1.call-update) | async-done | bytes 1048592 | tf_op jit(solution)/shard_map/reduce_scatter | solution.py:125
  293.9 0.0 copy-done.1
  (27 shorter events, 0.2 us)
Async XLA Ops:
  6.5 1.2 copy-start
  6.5 4.9 %copy-start.7 = (bf16[2048,256]{1,0:T(8,128)(2,1)S(1)}, bf16[2048,256]{1,0:T(8,128)(2,1)}, u32[]{:S(2)}) copy-start(bf16[2048,256]{1,0:T(8,128)(2,1)} %param.17) | copy-start | bytes 3145732
  6.5 135.2 %all-gather.2.cloned.1.call-start = ((), (), s32[]{:S(2)}) async-start(), calls=%async_computation.1 | async-start | bytes 9437184 | tf_op jit(solution)/shard_map/all_gather | solution.py:67
  7.8 3.6 %copy-start.5 = (bf16[1024,2048]{1,0:T(8,128)(2,1)S(1)}, bf16[1024,2048]{1,0:T(8,128)(2,1)}, u32[]{:S(2)}) copy-start(bf16[1024,2048]{1,0:T(8,128)(2,1)} %param.14) | copy-start | bytes 12582916
  11.4 2.4 copy-start.8
  12.7 4.8 %copy-start.9 = (bf16[2048,256]{1,0:T(8,128)(2,1)S(1)}, bf16[2048,256]{1,0:T(8,128)(2,1)}, u32[]{:S(2)}) copy-start(bf16[2048,256]{1,0:T(8,128)(2,1)} %param.18) | copy-start | bytes 3145732
  13.8 280.1 %reduce-scatter.2.cloned.1.call-start = ((), (), s32[]{:S(2)}) async-start(), calls=%async_computation.2 | async-start | bytes 5242880 | tf_op jit(solution)/shard_map/reduce_scatter | solution.py:125
  13.9 3.6 %copy-start.6 = (bf16[1024,2048]{1,0:T(8,128)(2,1)S(1)}, bf16[1024,2048]{1,0:T(8,128)(2,1)}, u32[]{:S(2)}) copy-start(bf16[1024,2048]{1,0:T(8,128)(2,1)} %param.14) | copy-start | bytes 12582916
  18.8 9.5 %copy-start.3 = (f32[31,256]{1,0:T(8,128)S(1)}, f32[31,256]{1,0:T(8,128)}, u32[]{:S(2)}) copy-start(f32[31,256]{1,0:T(8,128)} %param.20) | copy-start | bytes 95236
  18.8 9.5 %copy-start.2 = (f32[1024,2]{0,1:T(2,128)S(1)}, f32[1024,2]{0,1:T(2,128)}, u32[]{:S(2)}) copy-start(f32[1024,2]{0,1:T(2,128)} %param.22) | copy-start | bytes 24580
  18.8 42.0 %collective-permute-start = (bf16[30,256]{1,0:T(8,128)(2,1)S(1)}, bf16[30,256]{1,0:T(8,128)(2,1)S(1)}, u32[]{:S(2)}, u32[]{:S(2)}) collective-permute-start(bf16[30,256]{1,0:T(8,128)(2,1)S(1)} %slice.252), channel_id=1, source_target_pairs={{0,4},{4,8},{8,12},{12,16},{16,20},{20,24},{24,28},{1,5},{5,9},{9,... | collective-permute-start | bytes 46088 | tf_op jit(solution)/shard_map/ppermute | solution.py:14
  61.0 17.3 %copy-start.4 = (f32[256]{0:T(256)S(1)}, f32[256]{0:T(256)}, u32[]{:S(2)}) copy-start(f32[256]{0:T(256)} %param.21) | copy-start | bytes 3076
  160.6 133.3 %copy-start.1 = (bf16[2048,256]{1,0:T(8,128)(2,1)S(1)}, bf16[2048,256]{1,0:T(8,128)(2,1)}, u32[]{:S(2)}) copy-start(bf16[2048,256]{1,0:T(8,128)(2,1)} %param.16) | copy-start | bytes 3145732
Sparse Core Ops, SparseCore 0:
  13.9 127.7 all-gather.1
  167.8 126.0 reduce-scatter.1
